TPU v7x, 32 devices: a whole 2x2x4 slice. The times are simulated.
32 devices in a mesh: ep: 8 (over z, y), tp: 4 (over x, core).
Axes of the slice: x: 2, y: 2, z: 4, core: 2. Of those that a mesh axis runs over, the one named last changes fastest.
Arguments:
- queries: bfloat16 [2048, 1024], P('ep', 'tp'), may hold values from -200 to 200
- keys: bfloat16 [2048, 512], P('ep', 'tp'), may hold values from -5 to 5
- values: bfloat16 [2048, 512], P('ep', 'tp'), may hold values from -6 to 6
- log_gates: float32 [2048, 16], P('ep', 'tp'), may hold values from -2048 to 0, as said below
- out_weight: bfloat16 [1024, 2048], P('tp'), may hold values from -0.1875 to 0.1875
- moe_rows: bfloat16 [2048, 2048], P('ep'), may hold values from -6 to 6
- norm_gain: float32 [2048], replicated, may hold values from 0.1 to 1.9
- experts: int32 [2048, 2], P('ep'), may hold values from 0 to 7, all different within a row; in each aligned block of 256 rows (0 to 255, 256 to 511, ...) at most 128 rows name the same one
- expert_weights: float32 [2048, 2], P('ep'), may hold values from 0.2 to 1
- w_gate: bfloat16 [8, 2048, 1024], P('ep', None, 'tp'), may hold values from -0.125 to 0.125
- w_up: bfloat16 [8, 2048, 1024], P('ep', None, 'tp'), may hold values from -0.125 to 0.125
- w_down: bfloat16 [8, 1024, 2048], P('ep', 'tp'), may hold values from -0.1875 to 0.1875
Outputs:
- mixed: bfloat16 [2048, 2048], P(('ep', 'tp'))
- moe_out: bfloat16 [2048, 2048], P('ep', 'tp')
Inputs may be any that keep to these rules, and one draw needn't show every extreme that they name: Each token names 2 different experts; within the rows of one index of ep (aligned blocks of 256 rows) no expert is named more than 128 times, a bound that some block reaches. `log_gates`: Non-increasing along positions in every head.
All inputs are finite; a program needn't handle non-finite values.
Results may differ from a plain program's by a relative error of at most 0.01195.
Values may be sent and summed in bfloat16 or wider, within the bound.
A program may use at most 128 MiB of HBM per device.

v0:
```python
import math
import jax
import jax.numpy as jnp
from jax import lax
from jax.sharding import PartitionSpec as P

D = 2048
HD = 64
EPSILON = 1e-06
MASKED = -1e30


def prepare_group(query_rows, gate_rows, positions, kv_here, group):
    rows = query_rows.shape[0]
    query_heads = query_rows.reshape(rows, kv_here, group, HD)
    query_gates = jnp.transpose(gate_rows.reshape(rows, kv_here, group), (1, 2, 0))
    return (query_heads, query_gates, positions)


def empty_state(rows, kv_here, group):
    return (
        jnp.full((kv_here, group, rows), MASKED, jnp.float32),
        jnp.zeros((kv_here, group, rows), jnp.float32),
        jnp.zeros((kv_here, group, rows, HD), jnp.float32),
    )


def attend_group(prepared, state, key_part, value_part, gate_part, offset, kv_here, group):
    query_heads, query_gates, query_position = prepared
    length = key_part.shape[0]
    key_span = math.gcd(length, 512)

    def run_blocks(start_state):

        def one_block(turn_index, inner):
            running_max, running_sum, weighted = inner
            first = turn_index * key_span
            key_block = lax.dynamic_slice_in_dim(key_part, first, key_span, 0).reshape(
                key_span, kv_here, HD
            )
            value_block = lax.dynamic_slice_in_dim(value_part, first, key_span, 0).reshape(
                key_span, kv_here, HD
            )
            gate_block = lax.dynamic_slice_in_dim(gate_part, first, key_span, 0).reshape(
                key_span, kv_here, group
            )
            scores = jnp.einsum(
                "qgrd,kgd->grqk", query_heads, key_block, preferred_element_type=jnp.float32
            ) * HD ** (-0.5)
            scores = (
                scores
                + query_gates[..., None]
                - jnp.transpose(gate_block, (1, 2, 0))[:, :, None, :]
            )
            key_position = first + jnp.arange(key_span, dtype=jnp.int32)
            scores = jnp.where(key_position[None, :] <= query_position[:, None], scores, MASKED)
            new_max = jnp.maximum(running_max, jnp.max(scores, axis=-1))
            weights = jnp.exp(scores - new_max[..., None])
            rescale = jnp.exp(running_max - new_max)
            running_sum = running_sum * rescale + jnp.sum(weights, axis=-1)
            weighted = weighted * rescale[..., None] + jnp.einsum(
                "grqk,kgd->grqd",
                weights.astype(jnp.bfloat16),
                value_block,
                preferred_element_type=jnp.float32,
            )
            return (new_max, running_sum, weighted)

        return lax.fori_loop(0, length // key_span, one_block, start_state)

    def keep_state(start_state):
        return start_state

    return lax.cond(offset <= query_position[-1], run_blocks, keep_state, state)


def finish_group(state, heads_here):
    running_max, running_sum, weighted = state
    rows = weighted.shape[2]
    attended = weighted / running_sum[..., None]
    return jnp.transpose(attended, (2, 0, 1, 3)).reshape(rows, heads_here * HD).astype(jnp.bfloat16)


def mixer_half(queries, keys, values, log_gates, out_weight):
    tok_rows = queries.shape[0]
    heads_here = log_gates.shape[1]
    kv_here = keys.shape[1] // HD
    group = heads_here // kv_here
    own_index = lax.axis_index("ep")
    positions = own_index * tok_rows + jnp.arange(tok_rows, dtype=jnp.int32)
    groups = [prepare_group(queries, log_gates, positions, kv_here, group)]
    initial = tuple((empty_state(entry[0].shape[0], kv_here, group) for entry in groups))
    offset = jnp.int32(0)
    key_part = lax.all_gather(keys.astype(jnp.float32), "ep", axis=0, tiled=True).astype(
        jnp.bfloat16
    )
    value_part = lax.all_gather(values.astype(jnp.float32), "ep", axis=0, tiled=True).astype(
        jnp.bfloat16
    )
    gate_part = lax.all_gather(log_gates, "ep", axis=0, tiled=True)
    states = tuple(
        (
            attend_group(
                groups[number],
                initial[number],
                key_part,
                value_part,
                gate_part,
                offset,
                kv_here,
                group,
            )
            for number in range(len(groups))
        )
    )
    finished = [finish_group(state, heads_here) for state in states]
    attended = finished[0]
    return lax.psum_scatter(
        jnp.dot(attended, out_weight, preferred_element_type=jnp.float32).astype(jnp.bfloat16),
        "tp",
        scatter_dimension=0,
        tiled=True,
    )


def experts_half(moe_rows, norm_gain, experts, expert_weights, w_gate, w_up, w_down):
    rows_here = moe_rows.shape[0]
    topk = experts.shape[1]
    experts_all = lax.axis_size("ep")
    capacity = 4 * rows_here // experts_all
    rows_float = moe_rows.astype(jnp.float32)
    normed = (
        rows_float
        * lax.rsqrt(jnp.mean(rows_float * rows_float, axis=-1, keepdims=True) + EPSILON)
        * norm_gain
    ).astype(jnp.bfloat16)
    expert_ids = experts.reshape(-1)
    one_hot = (expert_ids[:, None] == jnp.arange(experts_all, dtype=jnp.int32)[None, :]).astype(
        jnp.int32
    )
    ranks = jnp.cumsum(one_hot, axis=0) - 1
    slot_index = jnp.sum(one_hot * ranks, axis=1)
    destination = expert_ids * capacity + slot_index
    token_index = jnp.arange(rows_here * topk, dtype=jnp.int32) // topk
    width = D // lax.axis_size("tp")
    source_rows = lax.dynamic_slice_in_dim(normed, lax.axis_index("tp") * width, width, 1)
    outgoing = jnp.zeros((experts_all * capacity, source_rows.shape[1]), jnp.bfloat16)
    outgoing = (
        outgoing.at[destination]
        .set(source_rows[token_index])
        .reshape(experts_all, capacity, source_rows.shape[1])
    )
    arrived = lax.all_to_all(outgoing, "ep", split_axis=0, concat_axis=0, tiled=True)
    arrived = lax.all_gather(arrived, "tp", axis=2, tiled=True)
    slots = arrived.shape[1]
    flat_rows = arrived.reshape(-1, D)
    gate_part = jnp.dot(flat_rows, w_gate[0], preferred_element_type=jnp.float32)
    up_part = jnp.dot(flat_rows, w_up[0], preferred_element_type=jnp.float32)
    hidden = (jax.nn.silu(gate_part) * up_part).astype(jnp.bfloat16)
    partial_out = jnp.dot(hidden, w_down[0], preferred_element_type=jnp.float32).reshape(
        experts_all, slots, D
    )
    summed = lax.psum_scatter(
        partial_out.astype(jnp.bfloat16), "tp", scatter_dimension=2, tiled=True
    )
    returned = lax.all_to_all(summed, "ep", split_axis=0, concat_axis=0, tiled=True)
    picked = returned.reshape(experts_all * capacity, -1)[destination].reshape(rows_here, topk, -1)
    return jnp.einsum("tk,tkd->td", expert_weights, picked.astype(jnp.float32)).astype(jnp.bfloat16)


def per_device(
    queries,
    keys,
    values,
    log_gates,
    out_weight,
    moe_rows,
    norm_gain,
    experts,
    expert_weights,
    w_gate,
    w_up,
    w_down,
):
    mixed = mixer_half(queries, keys, values, log_gates, out_weight)
    moe_out = experts_half(moe_rows, norm_gain, experts, expert_weights, w_gate, w_up, w_down)
    return (mixed, moe_out)


def solution(mesh):
    placed = (
        P("ep", "tp"),
        P("ep", "tp"),
        P("ep", "tp"),
        P("ep", "tp"),
        P("tp", None),
        P("ep", None),
        P(),
        P("ep", None),
        P("ep", None),
        P("ep", None, "tp"),
        P("ep", None, "tp"),
        P("ep", "tp", None),
    )
    return jax.shard_map(
        per_device,
        mesh=mesh,
        in_specs=placed,
        out_specs=(P(("ep", "tp"), None), P("ep", "tp")),
        check_vma=False,
    )
```

profile of v0, /device:TPU:0, one launch (start us, length us, event | category | flops | bytes accessed | tf_op | source)
XLA Modules:
  0.0 255.8 jit_solution(16764527390459552446)
XLA Ops:
  7.2 3.0 %convert_element_type.69 = f32[256,2048]{1,0:T(8,128)} convert(bf16[256,2048]{1,0:T(8,128)(2,1)} %param.21) | non-fusion elementwise | flops 524288 | bytes 3145728 | tf_op jit(solution)/shard_map/convert_element_type | solution.py:131
  11.0 1.1 reduce-window.6
  13.6 1.2 fusion.14
  14.7 5.0 %scatter_custom_fusion = bf16[1024,512]{1,0:T(8,128)(2,1)S(1)} fusion(s32[512]{0:T(512)S(1)} %bitcast.85, bf16[256,512]{1,0:T(8,128)(2,1)S(1)} %fusion.14, s32[1024]{0:T(1024)S(1)} %pad_clamp_fusion.1, bf16[]{:T(256)} %constant.107.clone.1), kind=kCustom, calls=%fused_computation.35 | custom fusion | bytes 1048578 | tf_op jit(solution)/shard_map/scatter | solution.py:150
  19.8 33.0 %all_to_all.10 = bf16[8,128,512]{2,1,0:T(8,128)(2,1)} all-to-all(bf16[8,128,512]{2,1,0:T(8,128)(2,1)S(1)} %bitcast.78), channel_id=1, replica_groups=mesh['ep'=8,'tp'=4] {'ep'}, dimensions={0} | all-to-all | bytes 2097152 | tf_op jit(solution)/shard_map/all_to_all | solution.py:153
  52.9 33.6 %all-gather.2.cloned.1.call-done = bf16[8,128,2048]{2,1,0:T(8,128)(2,1)} async-done(((bf16[8,128,512]{2,1,0:T(8,128)(2,1)}), bf16[8,128,2048]{2,1,0:T(8,128)(2,1)}) %all-gather.2.cloned.1.call-update) | async-done | bytes 4194320 | tf_op jit(solution)/shard_map/all_gather | solution.py:154
  86.4 3.6 %fusion.11 = f32[1024,256]{1,0:T(8,128)S(1)} fusion(bf16[1024,2048]{1,0:T(8,128)(2,1)} %bitcast.91, bf16[1,2048,256]{2,1,0:T(8,128)(2,1)S(1)} %copy-done.9), kind=kOutput, calls=%fused_computation.29 | convolution fusion | flops 1073741824 | bytes 6291456 | tf_op jit(solution)/shard_map/dot_general | solution.py:157
  90.2 1.3 fusion.8
  91.5 3.2 %convolution_convert_fusion = bf16[8,128,2048]{2,1,0:T(8,128)(2,1)} fusion(bf16[8,128,256]{2,1,0:T(8,128)(2,1)S(1)} %bitcast.81, bf16[1,256,2048]{2,1,0:T(8,128)(2,1)S(1)} %copy-done), kind=kOutput, calls=%fused_computation.22 | convolution fusion | flops 1075838976 | bytes 5767168 | tf_op jit(solution)/shard_map/dot_general | solution.py:160
  97.0 30.7 %all_gather.13 = f32[2048,4]{0,1:T(4,128)S(1)} all-gather(f32[256,4]{0,1:T(4,128)S(1)} %copy-done.5), channel_id=1, replica_groups=mesh['ep'=8,'tp'=4] {'ep'}, dimensions={0}, use_global_device_ids=true | all-gather | bytes 36864 | tf_op jit(solution)/shard_map/all_gather | solution.py:100
  127.7 33.5 %all_gather.12 = bf16[2048,128]{0,1:T(8,128)(2,1)} all-gather(bf16[256,128]{0,1:T(8,128)(2,1)S(1)} %copy.20), channel_id=1, replica_groups=mesh['ep'=8,'tp'=4] {'ep'}, dimensions={0}, use_global_device_ids=true | all-gather | bytes 589824 | tf_op jit(solution)/shard_map/all_gather | solution.py:94
  161.2 33.4 %all_gather.14 = bf16[2048,128]{0,1:T(8,128)(2,1)} all-gather(bf16[256,128]{0,1:T(8,128)(2,1)S(1)} %copy.21), channel_id=1, replica_groups=mesh['ep'=8,'tp'=4] {'ep'}, dimensions={0}, use_global_device_ids=true | all-gather | bytes 589824 | tf_op jit(solution)/shard_map/all_gather | solution.py:97
  194.5 25.2 %conditional.1 = (f32[2,2,256]{2,1,0:T(2,128)}, f32[2,2,256,64]{2,3,1,0:T(8,128)}) conditional(s32[]{:T(128)} %bitcast.1, () %tuple.30, (bf16[256,256]{1,0:T(8,128)(2,1)S(1)}, s32[256]{0:T(256)S(1)}, bf16[2048,128]{0,1:T(8,128)(2,1)}, f32[2,2,256]{2,1,0:T(2,128)S(1)}, f32[2048,4]{0,1:T(4,128)S(1)}, /*index=5*/bf16[2048,128]{0,1:T(8,128)(2,1)}) %tuple.69), branch_computations={%region_0.0_spmd, %region_1.6_spmd} | conditional | flops 139269632 | bytes 8373587 | solution.py:74
  195.3 24.4 %while.17 = (s32[]{:T(128)}, f32[2,2,256]{2,1,0:T(2,128)S(1)}, f32[2,2,256]{2,1,0:T(2,128)}, f32[2,2,256,64]{2,3,1,0:T(8,128)}, s32[256]{0:T(256)S(1)}, /*index=...) while((s32[]{:T(128)}, f32[2,2,256]{2,1,0:T(2,128)S(1)}, ...), condition=%wide.region_5.5_spmd.clone, body=%wide.region_2.4_spmd.clone.sunk | while | flops 139269632 | bytes 8111307 | solution.py:69
  195.3 1.0 constant_dynamic-slice_fusion.6
  196.5 1.6 fusion.44
  199.0 1.2 convolution_add_fusion.2
  200.2 1.0 constant_dynamic-slice_fusion.6
  201.4 1.6 fusion.44
  203.3 1.3 fusion.47
  204.6 2.1 convolution_add_fusion.2
  206.7 1.0 constant_dynamic-slice_fusion.6
  207.9 1.6 fusion.44
  209.8 1.3 fusion.47
  211.1 2.1 convolution_add_fusion.2
  214.4 1.6 fusion.44
  216.3 1.3 fusion.47
  217.6 2.1 convolution_add_fusion.2
  220.7 2.7 %convolution_convert_fusion.1 = bf16[256,2048]{1,0:T(8,128)(2,1)} fusion(bf16[256,256]{0,1:T(8,128)(2,1)S(1)} %bitcast.80, bf16[256,2048]{1,0:T(8,128)(2,1)} %param.20), kind=kOutput, calls=%fused_computation.23 | convolution fusion | flops 268959744 | bytes 2228224 | tf_op jit(solution)/shard_map/dot_general | solution.py:119
  223.5 5.8 %all-to-all-start.1 = ((bf16[8,128,512]{2,1,0:T(8,128)(2,1)}), bf16[8,128,512]{2,1,0:T(8,128)(2,1)S(1)}, u32[]{:S(2)}, u32[]{:S(2)}) async-start(bf16[8,128,512]{2,1,0:T(8,128)(2,1)} %reduce-scatter.5.cloned.1.call-done), calls=%async_computation.3 | async-start | bytes 2097152 | tf_op jit(solution)/shard_map/all_to_all | solution.py:166
  229.4 16.2 %all-to-all-done.1 = bf16[8,128,512]{2,1,0:T(8,128)(2,1)S(1)} async-done(((bf16[8,128,512]{2,1,0:T(8,128)(2,1)}), bf16[8,128,512]{2,1,0:T(8,128)(2,1)S(1)}, u32[]{:S(2)}, u32[]{:S(2)}) %all-to-all-start.1) | async-done | bytes 1048608 | tf_op jit(solution)/shard_map/all_to_all | solution.py:166
  245.6 2.0 gather_fusion
  (92 shorter events, 11.1 us)
Async XLA Ops:
  7.2 84.3 %copy-start = (bf16[1,256,2048]{2,1,0:T(8,128)(2,1)S(1)}, bf16[1,256,2048]{2,1,0:T(8,128)(2,1)}, u32[]{:S(2)}) copy-start(bf16[1,256,2048]{2,1,0:T(8,128)(2,1)} %param.27) | copy-start | bytes 3145732
  7.2 3.0 %copy-start.1 = (bf16[256,2048]{1,0:T(8,128)(2,1)S(1)}, bf16[256,2048]{1,0:T(8,128)(2,1)}, u32[]{:S(2)}) copy-start(bf16[256,2048]{1,0:T(8,128)(2,1)} %param.21) | copy-start | bytes 3145732
  7.2 79.2 %all-gather.2.cloned.1.call-start = ((), (), s32[]{:S(2)}) async-start(), calls=%async_computation.5 | async-start | bytes 5242880 | tf_op jit(solution)/shard_map/all_gather | solution.py:154
  7.2 3.3 %copy-start.6 = (s32[256,2]{0,1:T(2,128)S(1)}, s32[256,2]{0,1:T(2,128)}, u32[]{:S(2)}) copy-start(s32[256,2]{0,1:T(2,128)} %param.23) | copy-start | bytes 6148
  14.7 71.7 %copy-start.9 = (bf16[1,2048,256]{2,1,0:T(8,128)(2,1)S(1)}, bf16[1,2048,256]{2,1,0:T(8,128)(2,1)}, u32[]{:S(2)}) copy-start(bf16[1,2048,256]{2,1,0:T(8,128)(2,1)} %param.25) | copy-start | bytes 3145732
  52.8 170.7 %reduce-scatter.5.cloned.1.call-start = ((), (), s32[]{:S(2)}) async-start(), calls=%async_computation.6 | async-start | bytes 5242880 | tf_op jit(solution)/shard_map/reduce_scatter | solution.py:163
  86.4 3.6 %copy-start.8 = (bf16[8,128,2048]{2,1,0:T(8,128)(2,1)S(1)}, bf16[8,128,2048]{2,1,0:T(8,128)(2,1)}, u32[]{:S(2)}) copy-start(bf16[8,128,2048]{2,1,0:T(8,128)(2,1)} %all-gather.2.cloned.1.call-done) | copy-start | bytes 12582916
  86.4 3.7 %copy-start.10 = (bf16[1,2048,256]{2,1,0:T(8,128)(2,1)S(1)}, bf16[1,2048,256]{2,1,0:T(8,128)(2,1)}, u32[]{:S(2)}) copy-start(bf16[1,2048,256]{2,1,0:T(8,128)(2,1)} %param.26) | copy-start | bytes 3145732
  94.7 0.8 copy-start.3
  94.7 1.0 copy-start.4
  94.7 1.1 copy-start.5
  94.7 99.9 %copy-start.2 = (bf16[256,256]{1,0:T(8,128)(2,1)S(1)}, bf16[256,256]{1,0:T(8,128)(2,1)}, u32[]{:S(2)}) copy-start(bf16[256,256]{1,0:T(8,128)(2,1)} %param.16) | copy-start | bytes 393220
  94.7 154.6 %reduce-scatter.3.cloned.1.call-start = ((), (), s32[]{:S(2)}) async-start(), calls=%async_computation.4 | async-start | bytes 1310720 | tf_op jit(solution)/shard_map/reduce_scatter | solution.py:118
  223.4 5.8 %copy-start.7 = (f32[256,2]{0,1:T(2,128)S(1)}, f32[256,2]{0,1:T(2,128)}, u32[]{:S(2)}) copy-start(f32[256,2]{0,1:T(2,128)} %param.24) | copy-start | bytes 6148
  223.5 22.2 %all-to-all-start.1 = ((bf16[8,128,512]{2,1,0:T(8,128)(2,1)}), bf16[8,128,512]{2,1,0:T(8,128)(2,1)S(1)}, u32[]{:S(2)}, u32[]{:S(2)}) async-start(bf16[8,128,512]{2,1,0:T(8,128)(2,1)} %reduce-scatter.5.cloned.1.call-done), calls=%async_computation.3 | async-start | bytes 2097152 | tf_op jit(solution)/shard_map/all_to_all | solution.py:166
Sparse Core Ops, SparseCore 0:
  52.9 33.4 all-gather.1
  94.8 44.3 reduce-scatter.4
  223.6 25.0 reduce-scatter.2
where the time goes:
time: 257 us; the launch traced here: 256 us
  blocking collectives  131 us (51%)
  waiting for transfers between devices  49.8 us (19%)
  matrix products  25.3 us (10%)
  local copies, waits for them, and re-layouts  16.4 us (6%)
  between operations  14.7 us (6%)
  other arithmetic  13 us (5%)
  starting transfers between devices  5.88 us (2%)
    all_gather x1, waiting for transfers between devices, experts_half(): arrived = lax.all_gather(arrived, 'tp', axis=2, tiled=True)  33.6 us
    all_gather x1, blocking collectives, mixer_half(): lax.all_gather(keys.astype(jnp.float32), 'ep', axis=0, tiled=True)  33.5 us
    all_gather x1, blocking collectives, mixer_half(): lax.all_gather(values.astype(jnp.float32), 'ep', axis=0, tiled=True)  33.4 us
    all_to_all x1, blocking collectives, experts_half(): lax.all_to_all(outgoing, 'ep', split_axis=0, concat_axis=0, tiled=True)  33 us
    all_gather x1, blocking collectives, mixer_half(): gate_part = lax.all_gather(log_gates, 'ep', axis=0, tiled=True)  30.7 us
    all_to_all x1, waiting for transfers between devices, experts_half(): lax.all_to_all(summed, 'ep', split_axis=0, concat_axis=0, tiled=True)  16.2 us
    dot_general x4, matrix products, one_block(): jnp.einsum('grqk,kgd->grqd', weights.astype(jnp.bfloat16), value_block, p...  7.5 us
    dot_general x4, matrix products, one_block(): jnp.einsum('qgrd,kgd->grqk', query_heads, key_block, preferred_element_ty...  6.37 us
  transfers between devices with their start and end apart: 4, of which 2 were waited for; matrix products, arithmetic and copies ran while one was open for 13% of the time, Pallas kernels for 0%

commit v1 on v0

--- a/solution.py
+++ b/solution.py
@@ -8,6 +8,17 @@
 HD = 64
 EPSILON = 1e-06
 MASKED = -1e30
+
+
+def cut_along(array, dim, peers):
+    before, after = (array.shape[:dim], array.shape[dim + 1 :])
+    return jnp.moveaxis(array.reshape(*before, peers, -1, *after), dim, 0)
+
+
+def laid_out(blocks, dim):
+    lengths = list(blocks.shape[1:])
+    lengths[dim] *= blocks.shape[0]
+    return jnp.moveaxis(blocks, 0, dim).reshape(lengths)
 
 
 def prepare_group(query_rows, gate_rows, positions, kv_here, group):
@@ -150,7 +161,14 @@
         .set(source_rows[token_index])
         .reshape(experts_all, capacity, source_rows.shape[1])
     )
-    arrived = lax.all_to_all(outgoing, "ep", split_axis=0, concat_axis=0, tiled=True)
+    count, index = (lax.axis_size("ep"), lax.axis_index("ep"))
+    blocks = cut_along(outgoing, 0, count)
+    gathered = [blocks[index]]
+    for step in range(1, count):
+        sent = blocks[(index + step) % count]
+        gathered.append(lax.ppermute(sent, "ep", [(i, (i + step) % count) for i in range(count)]))
+    blocks = jnp.stack(gathered)[(index - jnp.arange(count)) % count]
+    arrived = laid_out(blocks, 0)
     arrived = lax.all_gather(arrived, "tp", axis=2, tiled=True)
     slots = arrived.shape[1]
     flat_rows = arrived.reshape(-1, D)

time: 257 us -> 255 us (level)
  blocking collectives: 131 us -> 97.5 us
  waiting for transfers between devices: 49.8 us -> 65.1 us
  starting transfers between devices: 5.88 us -> 20.3 us
    all_to_all x1 -> x0, blocking collectives: 33 us -> none  [experts_half(): lax.all_to_all(outgoing, 'ep', split_axis=0, concat_axis=0, tiled=True)]
    ppermute x0 -> x7, starting transfers between devices: none -> 14.4 us  [experts_half(): lax.ppermute(sent, 'ep', [(i, (i + step) % count) for i in range(count)])]
    all_gather x1, waiting for transfers between devices: 33.6 us -> 42 us  [experts_half(): arrived = lax.all_gather(arrived, 'tp', axis=2, tiled=True)]
    ppermute x0 -> x7, waiting for transfers between devices: none -> 6.81 us  [experts_half(): lax.ppermute(sent, 'ep', [(i, (i + step) % count) for i in range(count)])]
  transfers between devices with their start and end apart: 4 -> 11, of which waited for: 2 -> 4; matrix products, arithmetic and copies ran while one was open for 13% -> 13% of each run, Pallas kernels for 0% -> 0%
where the time goes in v1:
time: 255 us; the launch traced here: 254 us
  blocking collectives  97.5 us (38%)
  waiting for transfers between devices  65.1 us (26%)
  matrix products  25.3 us (10%)
  starting transfers between devices  20.3 us (8%)
  local copies, waits for them, and re-layouts  18.1 us (7%)
  between operations  14.9 us (6%)
  other arithmetic  13 us (5%)
    all_gather x1, waiting for transfers between devices, experts_half(): arrived = lax.all_gather(arrived, 'tp', axis=2, tiled=True)  42 us
    all_gather x1, blocking collectives, mixer_half(): lax.all_gather(keys.astype(jnp.float32), 'ep', axis=0, tiled=True)  33.5 us
    all_gather x1, blocking collectives, mixer_half(): lax.all_gather(values.astype(jnp.float32), 'ep', axis=0, tiled=True)  33.4 us
    all_gather x1, blocking collectives, mixer_half(): gate_part = lax.all_gather(log_gates, 'ep', axis=0, tiled=True)  30.7 us
    all_to_all x1, waiting for transfers between devices, experts_half(): lax.all_to_all(summed, 'ep', split_axis=0, concat_axis=0, tiled=True)  16.2 us
    ppermute x7, starting transfers between devices, experts_half(): lax.ppermute(sent, 'ep', [(i, (i + step) % count) for i in range(count)])  14.4 us
    dot_general x4, matrix products, one_block(): jnp.einsum('grqk,kgd->grqd', weights.astype(jnp.bfloat16), value_block, p...  7.48 us
    ppermute x7, waiting for transfers between devices, experts_half(): lax.ppermute(sent, 'ep', [(i, (i + step) % count) for i in range(count)])  6.81 us
  transfers between devices with their start and end apart: 11, of which 4 were waited for; matrix products, arithmetic and copies ran while one was open for 13% of the time, Pallas kernels for 0%

profile of v1, /device:TPU:0, one launch (start us, length us, event | category | flops | bytes accessed | tf_op | source)
XLA Modules:
  0.0 254.3 jit_solution(12733820807935180615)
XLA Ops:
  7.3 2.9 %convert_element_type.69 = f32[256,2048]{1,0:T(8,128)} convert(bf16[256,2048]{1,0:T(8,128)(2,1)} %param.21) | non-fusion elementwise | flops 524288 | bytes 3145728 | tf_op jit(solution)/shard_map/convert_element_type | solution.py:142
  14.8 5.0 %scatter_custom_fusion = bf16[1024,512]{1,0:T(8,128)(2,1)S(1)} fusion(s32[512]{0:T(512)S(1)} %bitcast.117, bf16[256,512]{1,0:T(8,128)(2,1)S(1)} %fusion.14, s32[1024]{0:T(1024)S(1)} %pad_clamp_fusion.2, bf16[]{:T(256)} %constant.157.clone.1), kind=kCustom, calls=%fused_computation.36 | custom fusion | bytes 1048578 | tf_op jit(solution)/shard_map/scatter | solution.py:161
  20.0 3.0 %collective-permute-start = (bf16[1,128,512]{2,1,0:T(8,128)(2,1)S(1)}, bf16[1,128,512]{2,1,0:T(8,128)(2,1)S(1)}, u32[]{:S(2)}, u32[]{:S(2)}) collective-permute-start(bf16[1,128,512]{2,1,0:T(8,128)(2,1)S(1)} %get-tuple-element.274), channel_id=1, source_target_pairs={{0,4},{4,8},{8,12},{12,16},{16,20},{20,24},{24,28},{28,0},{1,5},{5... | collective-permute-start | bytes 393224 | tf_op jit(solution)/shard_map/ppermute | solution.py:169
  23.1 1.6 collective-permute-start.1
  24.6 2.5 collective-permute-start.2
  28.4 2.6 %collective-permute-start.4 = (bf16[1,128,512]{2,1,0:T(8,128)(2,1)S(1)}, bf16[1,128,512]{2,1,0:T(8,128)(2,1)S(1)}, u32[]{:S(2)}, u32[]{:S(2)}) collective-permute-start(bf16[1,128,512]{2,1,0:T(8,128)(2,1)S(1)} %get-tuple-element.270), channel_id=1, source_target_pairs={{0,20},{4,24},{8,28},{12,0},{16,4},{20,8},{24,12},{28,16},{1,21},{... | collective-permute-start | bytes 393224 | tf_op jit(solution)/shard_map/ppermute | solution.py:169
  31.1 1.4 collective-permute-start.5
  32.5 2.0 collective-permute-start.6
  34.5 6.5 %collective-permute-done.2 = bf16[1,128,512]{2,1,0:T(8,128)(2,1)S(1)} collective-permute-done((bf16[1,128,512]{2,1,0:T(8,128)(2,1)S(1)}, bf16[1,128,512]{2,1,0:T(8,128)(2,1)S(1)}, u32[]{:S(2)}, u32[]{:S(2)}) %collective-permute-start.2) | collective-permute-done | bytes 131104 | tf_op jit(solution)/shard_map/ppermute | solution.py:169
  41.4 1.6 gather_fusion
  43.0 42.0 %all-gather.3.cloned.1.call-done = bf16[8,128,2048]{2,1,0:T(8,128)(2,1)} async-done(((bf16[8,128,512]{2,1,0:T(8,128)(2,1)}), bf16[8,128,2048]{2,1,0:T(8,128)(2,1)}) %all-gather.3.cloned.1.call-update) | async-done | bytes 4194320 | tf_op jit(solution)/shard_map/all_gather | solution.py:172
  85.0 3.6 %fusion.11 = f32[1024,256]{1,0:T(8,128)S(1)} fusion(bf16[1024,2048]{1,0:T(8,128)(2,1)} %bitcast.123, bf16[1,2048,256]{2,1,0:T(8,128)(2,1)S(1)} %copy-done.9), kind=kOutput, calls=%fused_computation.30 | convolution fusion | flops 1073741824 | bytes 6291456 | tf_op jit(solution)/shard_map/dot_general | solution.py:175
  90.1 3.2 %convolution_convert_fusion = bf16[8,128,2048]{2,1,0:T(8,128)(2,1)} fusion(bf16[8,128,256]{2,1,0:T(8,128)(2,1)S(1)} %bitcast.113, bf16[1,256,2048]{2,1,0:T(8,128)(2,1)S(1)} %copy-done), kind=kOutput, calls=%fused_computation.23 | convolution fusion | flops 1075838976 | bytes 5767168 | tf_op jit(solution)/shard_map/dot_general | solution.py:178
  95.6 30.7 %all_gather.13 = f32[2048,4]{0,1:T(4,128)S(1)} all-gather(f32[256,4]{0,1:T(4,128)S(1)} %copy-done.5), channel_id=1, replica_groups=mesh['ep'=8,'tp'=4] {'ep'}, dimensions={0}, use_global_device_ids=true | all-gather | bytes 36864 | tf_op jit(solution)/shard_map/all_gather | solution.py:111
  126.3 33.5 %all_gather.12 = bf16[2048,128]{0,1:T(8,128)(2,1)} all-gather(bf16[256,128]{0,1:T(8,128)(2,1)S(1)} %copy.20), channel_id=1, replica_groups=mesh['ep'=8,'tp'=4] {'ep'}, dimensions={0}, use_global_device_ids=true | all-gather | bytes 589824 | tf_op jit(solution)/shard_map/all_gather | solution.py:105
  159.8 33.4 %all_gather.14 = bf16[2048,128]{0,1:T(8,128)(2,1)} all-gather(bf16[256,128]{0,1:T(8,128)(2,1)S(1)} %copy.21), channel_id=1, replica_groups=mesh['ep'=8,'tp'=4] {'ep'}, dimensions={0}, use_global_device_ids=true | all-gather | bytes 589824 | tf_op jit(solution)/shard_map/all_gather | solution.py:108
  193.2 25.1 %conditional.1 = (f32[2,2,256]{2,1,0:T(2,128)}, f32[2,2,256,64]{2,3,1,0:T(8,128)}) conditional(s32[]{:T(128)} %bitcast.1, () %tuple.30, (bf16[256,256]{1,0:T(8,128)(2,1)S(1)}, s32[256]{0:T(256)S(1)}, bf16[2048,128]{0,1:T(8,128)(2,1)}, f32[2,2,256]{2,1,0:T(2,128)S(1)}, f32[2048,4]{0,1:T(4,128)S(1)}, /*index=5*/bf16[2048,128]{0,1:T(8,128)(2,1)}) %tuple.77), branch_computations={%region_0.0_spmd, %region_1.6_spmd} | conditional | flops 139269632 | bytes 8373587 | solution.py:85
  193.9 24.4 %while.17 = (s32[]{:T(128)}, f32[2,2,256]{2,1,0:T(2,128)S(1)}, f32[2,2,256]{2,1,0:T(2,128)}, f32[2,2,256,64]{2,3,1,0:T(8,128)}, s32[256]{0:T(256)S(1)}, /*index=...) while((s32[]{:T(128)}, f32[2,2,256]{2,1,0:T(2,128)S(1)}, ...), condition=%wide.region_5.5_spmd.clone, body=%wide.region_2.4_spmd.clone.sunk | while | flops 139269632 | bytes 8111307 | solution.py:80
  195.1 1.6 fusion.46
  200.0 1.6 fusion.46
  201.9 1.3 fusion.49
  203.2 2.1 convolution_add_fusion.2
  206.5 1.6 fusion.46
  208.4 1.3 fusion.49
  209.7 2.1 convolution_add_fusion.2
  213.0 1.6 fusion.46
  214.9 1.3 fusion.49
  216.2 2.1 convolution_add_fusion.2
  219.3 2.7 %convolution_convert_fusion.1 = bf16[256,2048]{1,0:T(8,128)(2,1)} fusion(bf16[256,256]{0,1:T(8,128)(2,1)S(1)} %bitcast.112, bf16[256,2048]{1,0:T(8,128)(2,1)} %param.20), kind=kOutput, calls=%fused_computation.24 | convolution fusion | flops 268959744 | bytes 2228224 | tf_op jit(solution)/shard_map/dot_general | solution.py:130
  222.0 5.8 %all-to-all-start = ((bf16[8,128,512]{2,1,0:T(8,128)(2,1)}), bf16[8,128,512]{2,1,0:T(8,128)(2,1)S(1)}, u32[]{:S(2)}, u32[]{:S(2)}) async-start(bf16[8,128,512]{2,1,0:T(8,128)(2,1)} %reduce-scatter.5.cloned.1.call-done), calls=%async_computation.2 | async-start | bytes 2097152 | tf_op jit(solution)/shard_map/all_to_all | solution.py:184
  228.0 16.2 %all-to-all-done = bf16[8,128,512]{2,1,0:T(8,128)(2,1)S(1)} async-done(((bf16[8,128,512]{2,1,0:T(8,128)(2,1)}), bf16[8,128,512]{2,1,0:T(8,128)(2,1)S(1)}, u32[]{:S(2)}, u32[]{:S(2)}) %all-to-all-start) | async-done | bytes 1048608 | tf_op jit(solution)/shard_map/all_to_all | solution.py:184
  244.2 2.0 gather_fusion.1
  (115 shorter events, 20.6 us)
Async XLA Ops:
  7.2 82.9 %copy-start = (bf16[1,256,2048]{2,1,0:T(8,128)(2,1)S(1)}, bf16[1,256,2048]{2,1,0:T(8,128)(2,1)}, u32[]{:S(2)}) copy-start(bf16[1,256,2048]{2,1,0:T(8,128)(2,1)} %param.27) | copy-start | bytes 3145732
  7.2 3.1 %copy-start.1 = (bf16[256,2048]{1,0:T(8,128)(2,1)S(1)}, bf16[256,2048]{1,0:T(8,128)(2,1)}, u32[]{:S(2)}) copy-start(bf16[256,2048]{1,0:T(8,128)(2,1)} %param.21) | copy-start | bytes 3145732
  7.2 77.8 %all-gather.3.cloned.1.call-start = ((), (), s32[]{:S(2)}) async-start(), calls=%async_computation.5 | async-start | bytes 5242880 | tf_op jit(solution)/shard_map/all_gather | solution.py:172
  7.3 3.2 %copy-start.6 = (s32[256,2]{0,1:T(2,128)S(1)}, s32[256,2]{0,1:T(2,128)}, u32[]{:S(2)}) copy-start(s32[256,2]{0,1:T(2,128)} %param.23) | copy-start | bytes 6148
  20.0 11.1 %collective-permute-start = (bf16[1,128,512]{2,1,0:T(8,128)(2,1)S(1)}, bf16[1,128,512]{2,1,0:T(8,128)(2,1)S(1)}, u32[]{:S(2)}, u32[]{:S(2)}) collective-permute-start(bf16[1,128,512]{2,1,0:T(8,128)(2,1)S(1)} %get-tuple-element.274), channel_id=1, source_target_pairs={{0,4},{4,8},{8,12},{12,16},{16,20},{20,24},{24,28},{28,0},{1,5},{5... | collective-permute-start | bytes 393224 | tf_op jit(solution)/shard_map/ppermute | solution.py:169
  23.1 9.4 %collective-permute-start.1 = (bf16[1,128,512]{2,1,0:T(8,128)(2,1)S(1)}, bf16[1,128,512]{2,1,0:T(8,128)(2,1)S(1)}, u32[]{:S(2)}, u32[]{:S(2)}) collective-permute-start(bf16[1,128,512]{2,1,0:T(8,128)(2,1)S(1)} %get-tuple-element.273), channel_id=1, source_target_pairs={{0,8},{4,12},{8,16},{12,20},{16,24},{20,28},{24,0},{28,4},{1,9},{5... | collective-permute-start | bytes 393224 | tf_op jit(solution)/shard_map/ppermute | solution.py:169
  24.6 16.3 %collective-permute-start.2 = (bf16[1,128,512]{2,1,0:T(8,128)(2,1)S(1)}, bf16[1,128,512]{2,1,0:T(8,128)(2,1)S(1)}, u32[]{:S(2)}, u32[]{:S(2)}) collective-permute-start(bf16[1,128,512]{2,1,0:T(8,128)(2,1)S(1)} %get-tuple-element.272), channel_id=1, source_target_pairs={{0,12},{4,16},{8,20},{12,24},{16,28},{20,0},{24,4},{28,8},{1,13},{... | collective-permute-start | bytes 393224 | tf_op jit(solution)/shard_map/ppermute | solution.py:169
  27.2 14.1 %collective-permute-start.3 = (bf16[1,128,512]{2,1,0:T(8,128)(2,1)S(1)}, bf16[1,128,512]{2,1,0:T(8,128)(2,1)S(1)}, u32[]{:S(2)}, u32[]{:S(2)}) collective-permute-start(bf16[1,128,512]{2,1,0:T(8,128)(2,1)S(1)} %get-tuple-element.271), channel_id=1, source_target_pairs={{0,16},{4,20},{8,24},{12,28},{16,0},{20,4},{24,8},{28,12},{1,17},{... | collective-permute-start | bytes 393224 | tf_op jit(solution)/shard_map/ppermute | solution.py:169
  28.4 12.9 %collective-permute-start.4 = (bf16[1,128,512]{2,1,0:T(8,128)(2,1)S(1)}, bf16[1,128,512]{2,1,0:T(8,128)(2,1)S(1)}, u32[]{:S(2)}, u32[]{:S(2)}) collective-permute-start(bf16[1,128,512]{2,1,0:T(8,128)(2,1)S(1)} %get-tuple-element.270), channel_id=1, source_target_pairs={{0,20},{4,24},{8,28},{12,0},{16,4},{20,8},{24,12},{28,16},{1,21},{... | collective-permute-start | bytes 393224 | tf_op jit(solution)/shard_map/ppermute | solution.py:169
  31.1 10.3 %collective-permute-start.5 = (bf16[1,128,512]{2,1,0:T(8,128)(2,1)S(1)}, bf16[1,128,512]{2,1,0:T(8,128)(2,1)S(1)}, u32[]{:S(2)}, u32[]{:S(2)}) collective-permute-start(bf16[1,128,512]{2,1,0:T(8,128)(2,1)S(1)} %get-tuple-element.269), channel_id=1, source_target_pairs={{0,24},{4,28},{8,0},{12,4},{16,8},{20,12},{24,16},{28,20},{1,25},{... | collective-permute-start | bytes 393224 | tf_op jit(solution)/shard_map/ppermute | solution.py:169
  32.5 8.9 %collective-permute-start.6 = (bf16[1,128,512]{2,1,0:T(8,128)(2,1)S(1)}, bf16[1,128,512]{2,1,0:T(8,128)(2,1)S(1)}, u32[]{:S(2)}, u32[]{:S(2)}) collective-permute-start(bf16[1,128,512]{2,1,0:T(8,128)(2,1)S(1)} %get-tuple-element.268), channel_id=1, source_target_pairs={{0,28},{4,0},{8,4},{12,8},{16,12},{20,16},{24,20},{28,24},{1,29},{... | collective-permute-start | bytes 393224 | tf_op jit(solution)/shard_map/ppermute | solution.py:169
  41.0 44.1 %copy-start.9 = (bf16[1,2048,256]{2,1,0:T(8,128)(2,1)S(1)}, bf16[1,2048,256]{2,1,0:T(8,128)(2,1)}, u32[]{:S(2)}) copy-start(bf16[1,2048,256]{2,1,0:T(8,128)(2,1)} %param.25) | copy-start | bytes 3145732
  43.0 179.0 %reduce-scatter.5.cloned.1.call-start = ((), (), s32[]{:S(2)}) async-start(), calls=%async_computation.4 | async-start | bytes 5242880 | tf_op jit(solution)/shard_map/reduce_scatter | solution.py:181
  85.0 3.6 %copy-start.8 = (bf16[8,128,2048]{2,1,0:T(8,128)(2,1)S(1)}, bf16[8,128,2048]{2,1,0:T(8,128)(2,1)}, u32[]{:S(2)}) copy-start(bf16[8,128,2048]{2,1,0:T(8,128)(2,1)} %all-gather.3.cloned.1.call-done) | copy-start | bytes 12582916
  85.0 3.7 %copy-start.10 = (bf16[1,2048,256]{2,1,0:T(8,128)(2,1)S(1)}, bf16[1,2048,256]{2,1,0:T(8,128)(2,1)}, u32[]{:S(2)}) copy-start(bf16[1,2048,256]{2,1,0:T(8,128)(2,1)} %param.26) | copy-start | bytes 3145732
  93.3 0.8 copy-start.3
  93.3 1.0 copy-start.4
  93.3 1.1 copy-start.5
  93.3 99.9 %copy-start.2 = (bf16[256,256]{1,0:T(8,128)(2,1)S(1)}, bf16[256,256]{1,0:T(8,128)(2,1)}, u32[]{:S(2)}) copy-start(bf16[256,256]{1,0:T(8,128)(2,1)} %param.16) | copy-start | bytes 393220
  93.3 154.5 %reduce-scatter.3.cloned.1.call-start = ((), (), s32[]{:S(2)}) async-start(), calls=%async_computation.3 | async-start | bytes 1310720 | tf_op jit(solution)/shard_map/reduce_scatter | solution.py:129
  222.0 5.8 %copy-start.7 = (f32[256,2]{0,1:T(2,128)S(1)}, f32[256,2]{0,1:T(2,128)}, u32[]{:S(2)}) copy-start(f32[256,2]{0,1:T(2,128)} %param.24) | copy-start | bytes 6148
  222.0 22.2 %all-to-all-start = ((bf16[8,128,512]{2,1,0:T(8,128)(2,1)}), bf16[8,128,512]{2,1,0:T(8,128)(2,1)S(1)}, u32[]{:S(2)}, u32[]{:S(2)}) async-start(bf16[8,128,512]{2,1,0:T(8,128)(2,1)} %reduce-scatter.5.cloned.1.call-done), calls=%async_computation.2 | async-start | bytes 2097152 | tf_op jit(solution)/shard_map/all_to_all | solution.py:184
Sparse Core Ops, SparseCore 0:
  43.1 41.8 all-gather.2
  93.4 44.3 reduce-scatter.4
  222.1 25.0 reduce-scatter.2
